TPU v7x, 32 devices: a whole 2x2x4 slice. The times are simulated.
32 devices in a mesh: rep: 4 (over z), fs: 4 (over y, x), tp: 2 (over core).
Axes of the slice: x: 2, y: 2, z: 4, core: 2. Of those that a mesh axis runs over, the one named last changes fastest.
Arguments:
- hidden_in: bfloat16 [2048, 2048], P('rep'), may hold values from -6 to 6
- cotangent: bfloat16 [2048, 2048], P('rep'), may hold values from -3 to 3
- w_up: bfloat16 [2048, 8192], P('rep', ('fs', 'tp')), may hold values from -0.125 to 0.125
- w_down: bfloat16 [8192, 2048], P(('fs', 'tp'), 'rep'), may hold values from -0.0625 to 0.0625
Outputs:
- input_grad: bfloat16 [2048, 2048], P('rep')
- up_grad: float32 [2048, 8192], P('rep', ('fs', 'tp'))
- down_grad: float32 [8192, 2048], P(('fs', 'tp'), 'rep')
All inputs are finite; a program needn't handle non-finite values.
Results may differ from a plain program's by a relative error of at most 0.017.
Values may be sent and summed in bfloat16 or wider, within the bound.
A program may use at most 64 MiB of HBM per device.

v0:
```python
import jax
import jax.numpy as jnp
from jax import lax
from jax.sharding import PartitionSpec as P


def contract_last(left, right):
    return lax.dot_general(
        left, right, (((1,), (1,)), ((), ())), preferred_element_type=jnp.float32
    )


def contract_first(left, right):
    return lax.dot_general(
        left, right, (((0,), (0,)), ((), ())), preferred_element_type=jnp.float32
    )


def on_device(hidden_in, cotangent, w_up, w_down):
    up_full = lax.all_gather(w_up, "rep", axis=0, tiled=True)
    back_grad = contract_last(cotangent, lax.all_gather(w_down, "rep", axis=1, tiled=True))
    preact = jnp.dot(hidden_in, up_full, preferred_element_type=jnp.float32)
    active = jnp.maximum(preact, 0.0)
    hidden = (active * active).astype(jnp.bfloat16)
    slopes = (2.0 * active * back_grad).astype(jnp.bfloat16)
    grad_upper = lax.psum_scatter(
        contract_first(hidden_in, slopes).astype(jnp.bfloat16),
        "rep",
        scatter_dimension=0,
        tiled=True,
    ).astype(jnp.float32)
    lower_rows = lax.psum_scatter(
        contract_first(cotangent, hidden).astype(jnp.bfloat16),
        "rep",
        scatter_dimension=0,
        tiled=True,
    ).astype(jnp.float32)
    down_grad = lower_rows.T
    partial_sum = contract_last(slopes, up_full).astype(jnp.bfloat16)
    input_grad = lax.psum(partial_sum, ("fs", "tp")).astype(jnp.float32).astype(jnp.bfloat16)
    return (input_grad, grad_upper, down_grad)


def solution(mesh):
    return jax.shard_map(
        on_device,
        mesh=mesh,
        in_specs=(P("rep", None), P("rep", None), P("rep", ("fs", "tp")), P(("fs", "tp"), "rep")),
        out_specs=(P("rep", None), P("rep", ("fs", "tp")), P(("fs", "tp"), "rep")),
        check_vma=False,
    )
```

profile of v0, /device:TPU:0, one launch (start us, length us, event | category | flops | bytes accessed | tf_op | source)
XLA Modules:
  0.0 414.7 jit_solution(14841434194789787365)
XLA Ops:
  7.2 0.0 copy-start
  7.2 0.0 all-gather.3.cloned.1.call-start
  7.2 0.7 all-gather.3.cloned.1.call-update
  7.9 0.0 all-gather.5.cloned.1.call-start
  8.0 0.7 all-gather.5.cloned.1.call-update
  8.7 0.0 reduce-scatter.3.cloned.1.call-start
  8.7 84.3 %all-gather.3.cloned.1.call-done = bf16[2048,1024]{1,0:T(8,128)(2,1)} async-done(((bf16[512,1024]{1,0:T(8,128)(2,1)}), bf16[2048,1024]{1,0:T(8,128)(2,1)}) %all-gather.3.cloned.1.call-update) | async-done | bytes 4194320 | tf_op jit(solution)/shard_map/all_gather | solution.py:20
  93.1 0.0 copy-done
  93.1 5.8 %fusion.2 = f32[512,1024]{1,0:T(8,128)} fusion(bf16[512,2048]{1,0:T(8,128)(2,1)S(1)} %copy-done, bf16[2048,1024]{1,0:T(8,128)(2,1)} %all-gather.3.cloned.1.call-done), kind=kOutput, calls=%fused_computation.8 | convolution fusion | flops 2147483648 | bytes 8388608 | tf_op jit(solution)/shard_map/dot_general | solution.py:22
  98.9 75.0 %all-gather.5.cloned.1.call-done = bf16[1024,2048]{1,0:T(8,128)(2,1)} async-done(((bf16[1024,512]{1,0:T(8,128)(2,1)}), bf16[1024,2048]{1,0:T(8,128)(2,1)}) %all-gather.5.cloned.1.call-update) | async-done | bytes 4194320 | tf_op jit(solution)/shard_map/all_gather | solution.py:21
  173.9 5.8 %multiply_convert_fusion.1 = bf16[512,1024]{1,0:T(8,128)(2,1)S(1)} fusion(f32[512,1024]{1,0:T(8,128)} %fusion.2, bf16[512,2048]{1,0:T(8,128)(2,1)} %param.5, bf16[1024,2048]{1,0:T(8,128)(2,1)} %all-gather.5.cloned.1.call-done), kind=kOutput, calls=%fused_computation.5 | convolution fusion | flops 2149580800 | bytes 9437184 | tf_op jit(solution)/shard_map/dot_general | solution.py:8
  179.7 4.4 %convert_bitcast_fusion.1 = bf16[2048,1024]{0,1:T(8,128)(2,1)} fusion(bf16[512,1024]{1,0:T(8,128)(2,1)S(1)} %multiply_convert_fusion.1, bf16[512,2048]{1,0:T(8,128)(2,1)S(1)} %copy-done), kind=kOutput, calls=%fused_computation.1 | convolution fusion | flops 2149580800 | bytes 7340032 | tf_op jit(solution)/shard_map/dot_general | solution.py:14
  184.1 0.0 reduce-scatter.3.cloned.1.call-update
  184.1 0.0 reduce-scatter.5.cloned.1.call-start
  184.2 6.6 %convert_bitcast_fusion = bf16[2048,1024]{0,1:T(8,128)(2,1)} fusion(bf16[512,2048]{1,0:T(8,128)(2,1)} %param.5, f32[512,1024]{1,0:T(8,128)} %fusion.2), kind=kOutput, calls=%fused_computation | convolution fusion | flops 2151153664 | bytes 8388608 | tf_op jit(solution)/shard_map/dot_general | solution.py:14
  190.8 0.0 reduce-scatter.5.cloned.1.call-update
  190.8 0.0 all-reduce.2.cloned.1.call-start
  190.8 5.9 %convolution_convert_fusion = bf16[512,2048]{1,0:T(8,128)(2,1)} fusion(bf16[512,1024]{1,0:T(8,128)(2,1)S(1)} %multiply_convert_fusion.1, bf16[2048,1024]{1,0:T(8,128)(2,1)} %all-gather.3.cloned.1.call-done), kind=kOutput, calls=%fused_computation.2 | convolution fusion | flops 2148532224 | bytes 7340032 | tf_op jit(solution)/shard_map/dot_general | solution.py:8
  196.7 0.0 all-reduce.2.cloned.1.call-update
  196.7 62.8 %reduce-scatter.3.cloned.1.call-done = bf16[512,1024]{0,1:T(8,128)(2,1)} async-done(((bf16[2048,1024]{0,1:T(8,128)(2,1)}), bf16[512,1024]{0,1:T(8,128)(2,1)}) %reduce-scatter.3.cloned.1.call-update) | async-done | bytes 1048592 | tf_op jit(solution)/shard_map/reduce_scatter | solution.py:26
  259.6 2.6 copy.7
  262.1 76.9 %reduce-scatter.5.cloned.1.call-done = bf16[512,1024]{0,1:T(8,128)(2,1)} async-done(((bf16[2048,1024]{0,1:T(8,128)(2,1)}), bf16[512,1024]{0,1:T(8,128)(2,1)}) %reduce-scatter.5.cloned.1.call-update) | async-done | bytes 1048592 | tf_op jit(solution)/shard_map/reduce_scatter | solution.py:32
  339.1 2.8 convert_bitcast_fusion.2
  341.9 63.1 %all-reduce.2.cloned.1.call-done = bf16[512,2048]{1,0:T(8,128)(2,1)} async-done(((bf16[512,2048]{1,0:T(8,128)(2,1)}), bf16[512,2048]{1,0:T(8,128)(2,1)}) %all-reduce.2.cloned.1.call-update) | async-done | bytes 2097168 | tf_op jit(solution)/shard_map/psum | solution.py:40
  405.0 3.2 copy.9
Async XLA Ops:
  7.2 85.9 %copy-start = (bf16[512,2048]{1,0:T(8,128)(2,1)S(1)}, bf16[512,2048]{1,0:T(8,128)(2,1)}, u32[]{:S(2)}) copy-start(bf16[512,2048]{1,0:T(8,128)(2,1)} %param.4) | copy-start | bytes 6291460
  7.2 85.9 %all-gather.3.cloned.1.call-start = ((), (), s32[]{:S(2)}) async-start(), calls=%async_computation.2 | async-start | bytes 5242880 | tf_op jit(solution)/shard_map/all_gather | solution.py:20
  7.9 166.0 %all-gather.5.cloned.1.call-start = ((), (), s32[]{:S(2)}) async-start(), calls=%async_computation.3 | async-start | bytes 5242880 | tf_op jit(solution)/shard_map/all_gather | solution.py:21
  8.7 250.9 %reduce-scatter.3.cloned.1.call-start = ((), (), s32[]{:S(2)}) async-start(), calls=%async_computation.5 | async-start | bytes 5242880 | tf_op jit(solution)/shard_map/reduce_scatter | solution.py:26
  184.1 154.9 %reduce-scatter.5.cloned.1.call-start = ((), (), s32[]{:S(2)}) async-start(), calls=%async_computation.6 | async-start | bytes 5242880 | tf_op jit(solution)/shard_map/reduce_scatter | solution.py:32
  190.8 214.2 %all-reduce.2.cloned.1.call-start = ((), (), s32[]{:S(2)}) async-start(), calls=%async_computation.4 | async-start | bytes 4194304 | tf_op jit(solution)/shard_map/psum | solution.py:40
Sparse Core Ops, SparseCore 0:
  9.6 83.4 all-gather.2
  94.6 79.2 all-gather.4
  184.3 75.2 reduce-scatter.2
  261.7 77.2 reduce-scatter.4
  342.7 62.2 all-reduce.1
where the time goes:
time: 415 us
  waiting for transfers between devices  364 us (88%)
  matrix products  28.5 us (7%)
  between operations  13.8 us (3%)
  local copies, waits for them, and re-layouts  5.73 us (1%)
    all_gather x1, waiting for transfers between devices, on_device(): up_full = lax.all_gather(w_up, 'rep', axis=0, tiled=True)  84.3 us
    reduce_scatter x1, waiting for transfers between devices, on_device(): lax.psum_scatter(contract_first(cotangent, hidden).astype(jnp.bfloat16),...  76.9 us
    all_gather x1, waiting for transfers between devices, on_device(): lax.all_gather(w_down, 'rep', axis=1, tiled=True)  75 us
    psum x1, waiting for transfers between devices, on_device(): lax.psum(partial_sum, ('fs', 'tp')).astype(jnp.float32).astype(jnp.bfloat16)  63.1 us
    reduce_scatter x1, waiting for transfers between devices, on_device(): lax.psum_scatter(contract_first(hidden_in, slopes).astype(jnp.bfloat16),...  62.8 us
    dot_general x2, matrix products, contract_last(): lax.dot_general(left, right, (((1,), (1,)), ((), ())), preferred_element_...  11.7 us
    dot_general x2, matrix products, contract_first(): lax.dot_general(left, right, (((0,), (0,)), ((), ())), preferred_element_...  10.9 us
  transfers between devices with their start and end apart: 5, of which 5 were waited for; matrix products, arithmetic and copies ran while one was open for 6% of the time, Pallas kernels for 0%

commit v1 on v0

--- a/solution.py
+++ b/solution.py
@@ -37,7 +37,9 @@
     ).astype(jnp.float32)
     down_grad = lower_rows.T
     partial_sum = contract_last(slopes, up_full).astype(jnp.bfloat16)
-    input_grad = lax.psum(partial_sum, ("fs", "tp")).astype(jnp.float32).astype(jnp.bfloat16)
+    input_grad = (
+        lax.psum(lax.psum(partial_sum, "tp"), "fs").astype(jnp.float32).astype(jnp.bfloat16)
+    )
     return (input_grad, grad_upper, down_grad)
 
 

time: 415 us -> 446 us (1.075)
  waiting for transfers between devices: 364 us -> 397 us
    reduce_scatter x1, waiting for transfers between devices: 62.8 us -> 80.1 us  [on_device(): lax.psum_scatter(contract_first(hidden_in, slopes).astype(jnp.bfloat16),...]
    psum x1 -> x2, waiting for transfers between devices: 63.1 us -> 78.9 us  [the longest x1 70.1 us: on_device(): lax.psum(lax.psum(partial_sum, 'tp'), 'fs').astype(jnp.float32)]
  transfers between devices with their start and end apart: 5 -> 6, of which waited for: 5 -> 6; matrix products, arithmetic and copies ran while one was open for 6% -> 5% of each run, Pallas kernels for 0% -> 0%
where the time goes in v1:
time: 446 us
  waiting for transfers between devices  397 us (89%)
  matrix products  26.5 us (6%)
  between operations  14.1 us (3%)
  local copies, waits for them, and re-layouts  5.73 us (1%)
    all_gather x1, waiting for transfers between devices, on_device(): up_full = lax.all_gather(w_up, 'rep', axis=0, tiled=True)  84.3 us
    reduce_scatter x1, waiting for transfers between devices, on_device(): lax.psum_scatter(contract_first(hidden_in, slopes).astype(jnp.bfloat16),...  80.1 us
    reduce_scatter x1, waiting for transfers between devices, on_device(): lax.psum_scatter(contract_first(cotangent, hidden).astype(jnp.bfloat16),...  76.9 us
    all_gather x1, waiting for transfers between devices, on_device(): lax.all_gather(w_down, 'rep', axis=1, tiled=True)  75 us
    psum x1, waiting for transfers between devices, on_device(): lax.psum(lax.psum(partial_sum, 'tp'), 'fs').astype(jnp.float32)  70.1 us
    dot_general x2, matrix products, contract_first(): lax.dot_general(left, right, (((0,), (0,)), ((), ())), preferred_element_...  11 us
    dot_general x2, matrix products, contract_last(): lax.dot_general(left, right, (((1,), (1,)), ((), ())), preferred_element_...  9.71 us
  transfers between devices with their start and end apart: 6, of which 6 were waited for; matrix products, arithmetic and copies ran while one was open for 5% of the time, Pallas kernels for 0%

profile of v1, /device:TPU:0, one launch (start us, length us, event | category | flops | bytes accessed | tf_op | source)
XLA Modules:
  0.0 446.2 jit_solution(2885865988723922395)
XLA Ops:
  7.2 0.0 copy-start
  7.2 0.0 all-gather.3.cloned.1.call-start
  7.2 0.7 all-gather.3.cloned.1.call-update
  7.9 0.0 all-gather.5.cloned.1.call-start
  8.0 0.7 all-gather.5.cloned.1.call-update
  8.7 0.0 all-reduce.3.cloned.1.call-start
  8.7 84.3 %all-gather.3.cloned.1.call-done = bf16[2048,1024]{1,0:T(8,128)(2,1)} async-done(((bf16[512,1024]{1,0:T(8,128)(2,1)}), bf16[2048,1024]{1,0:T(8,128)(2,1)}) %all-gather.3.cloned.1.call-update) | async-done | bytes 4194320 | tf_op jit(solution)/shard_map/all_gather | solution.py:20
  93.1 0.0 copy-done
  93.1 5.8 %fusion.2 = f32[512,1024]{1,0:T(8,128)} fusion(bf16[512,2048]{1,0:T(8,128)(2,1)S(1)} %copy-done, bf16[2048,1024]{1,0:T(8,128)(2,1)} %all-gather.3.cloned.1.call-done), kind=kOutput, calls=%fused_computation.8 | convolution fusion | flops 2147483648 | bytes 8388608 | tf_op jit(solution)/shard_map/dot_general | solution.py:22
  98.9 75.0 %all-gather.5.cloned.1.call-done = bf16[1024,2048]{1,0:T(8,128)(2,1)} async-done(((bf16[1024,512]{1,0:T(8,128)(2,1)}), bf16[1024,2048]{1,0:T(8,128)(2,1)}) %all-gather.5.cloned.1.call-update) | async-done | bytes 4194320 | tf_op jit(solution)/shard_map/all_gather | solution.py:21
  173.9 0.0 copy-start.1
  173.9 6.0 %multiply_convert_fusion.1 = bf16[512,1024]{1,0:T(8,128)(2,1)S(1)} fusion(f32[512,1024]{1,0:T(8,128)} %fusion.2, bf16[512,2048]{1,0:T(8,128)(2,1)} %param.5, bf16[1024,2048]{1,0:T(8,128)(2,1)} %all-gather.5.cloned.1.call-done), kind=kOutput, calls=%fused_computation.5 | convolution fusion | flops 2149580800 | bytes 9437184 | tf_op jit(solution)/shard_map/dot_general | solution.py:8
  179.9 0.0 copy-done.1
  179.9 3.7 convolution_convert_fusion
  183.6 0.0 all-reduce.3.cloned.1.call-update
  183.6 0.0 reduce-scatter.3.cloned.1.call-start
  183.7 4.3 convert_bitcast_fusion.1
  188.0 0.0 reduce-scatter.3.cloned.1.call-update
  188.0 0.0 reduce-scatter.5.cloned.1.call-start
  188.1 6.7 %convert_bitcast_fusion = bf16[2048,1024]{0,1:T(8,128)(2,1)} fusion(bf16[512,2048]{1,0:T(8,128)(2,1)} %param.5, f32[512,1024]{1,0:T(8,128)} %fusion.2), kind=kOutput, calls=%fused_computation | convolution fusion | flops 2151153664 | bytes 8388608 | tf_op jit(solution)/shard_map/dot_general | solution.py:14
  194.8 0.0 reduce-scatter.5.cloned.1.call-update
  194.8 0.0 all-reduce.5.cloned.1.call-start
  194.8 8.7 %all-reduce.3.cloned.1.call-done = bf16[512,2048]{1,0:T(8,128)(2,1)} async-done(((bf16[512,2048]{1,0:T(8,128)(2,1)}), bf16[512,2048]{1,0:T(8,128)(2,1)}) %all-reduce.3.cloned.1.call-update) | async-done | bytes 2097168 | tf_op jit(solution)/shard_map/psum | solution.py:41
  203.6 0.0 all-reduce.5.cloned.1.call-update
  203.6 80.1 %reduce-scatter.3.cloned.1.call-done = bf16[512,1024]{0,1:T(8,128)(2,1)} async-done(((bf16[2048,1024]{0,1:T(8,128)(2,1)}), bf16[512,1024]{0,1:T(8,128)(2,1)}) %reduce-scatter.3.cloned.1.call-update) | async-done | bytes 1048592 | tf_op jit(solution)/shard_map/reduce_scatter | solution.py:26
  283.7 2.6 copy.7
  286.3 76.9 %reduce-scatter.5.cloned.1.call-done = bf16[512,1024]{0,1:T(8,128)(2,1)} async-done(((bf16[2048,1024]{0,1:T(8,128)(2,1)}), bf16[512,1024]{0,1:T(8,128)(2,1)}) %reduce-scatter.5.cloned.1.call-update) | async-done | bytes 1048592 | tf_op jit(solution)/shard_map/reduce_scatter | solution.py:32
  363.2 2.8 convert_bitcast_fusion.2
  366.0 70.1 %all-reduce.5.cloned.1.call-done = bf16[512,2048]{1,0:T(8,128)(2,1)} async-done(((bf16[512,2048]{1,0:T(8,128)(2,1)}), bf16[512,2048]{1,0:T(8,128)(2,1)}) %all-reduce.5.cloned.1.call-update) | async-done | bytes 2097168 | tf_op jit(solution)/shard_map/psum | solution.py:41
  436.2 3.2 copy.10
Async XLA Ops:
  7.2 85.9 %copy-start = (bf16[512,2048]{1,0:T(8,128)(2,1)S(1)}, bf16[512,2048]{1,0:T(8,128)(2,1)}, u32[]{:S(2)}) copy-start(bf16[512,2048]{1,0:T(8,128)(2,1)} %param.4) | copy-start | bytes 6291460
  7.2 85.9 %all-gather.3.cloned.1.call-start = ((), (), s32[]{:S(2)}) async-start(), calls=%async_computation.2 | async-start | bytes 5242880 | tf_op jit(solution)/shard_map/all_gather | solution.py:20
  7.9 166.0 %all-gather.5.cloned.1.call-start = ((), (), s32[]{:S(2)}) async-start(), calls=%async_computation.3 | async-start | bytes 5242880 | tf_op jit(solution)/shard_map/all_gather | solution.py:21
  8.7 194.9 %all-reduce.3.cloned.1.call-start = ((), (), s32[]{:S(2)}) async-start(), calls=%async_computation.4 | async-start | bytes 4194304 | tf_op jit(solution)/shard_map/psum | solution.py:41
  173.9 6.0 %copy-start.1 = (bf16[2048,1024]{1,0:T(8,128)(2,1)S(1)}, bf16[2048,1024]{1,0:T(8,128)(2,1)}, u32[]{:S(2)}) copy-start(bf16[2048,1024]{1,0:T(8,128)(2,1)} %all-gather.3.cloned.1.call-done) | copy-start | bytes 12582916
  183.6 100.1 %reduce-scatter.3.cloned.1.call-start = ((), (), s32[]{:S(2)}) async-start(), calls=%async_computation.6 | async-start | bytes 5242880 | tf_op jit(solution)/shard_map/reduce_scatter | solution.py:26
  188.0 175.2 %reduce-scatter.5.cloned.1.call-start = ((), (), s32[]{:S(2)}) async-start(), calls=%async_computation.7 | async-start | bytes 5242880 | tf_op jit(solution)/shard_map/reduce_scatter | solution.py:32
  194.8 241.4 %all-reduce.5.cloned.1.call-start = ((), (), s32[]{:S(2)}) async-start(), calls=%async_computation.5 | async-start | bytes 4194304 | tf_op jit(solution)/shard_map/psum | solution.py:41
Sparse Core Ops, SparseCore 0:
  9.6 83.4 all-gather.2
  94.6 79.2 all-gather.4
  183.8 19.7 all-reduce.2
  205.7 77.9 reduce-scatter.2
  285.8 77.2 reduce-scatter.4
  366.1 69.9 all-reduce.4
